TPU v7x, 32 devices: a whole 2x2x4 slice. The times are simulated.
32 devices in a mesh: ep: 8 (over z, x), tp: 4 (over y, core).
Axes of the slice: x: 2, y: 2, z: 4, core: 2. Of those that a mesh axis runs over, the one named last changes fastest.
Arguments:
- mix_query: bfloat16 [16384, 2048], P('ep', 'tp'), may hold values from -6 to 6
- mix_key: bfloat16 [16384, 2048], P('ep', 'tp'), may hold values from -6 to 6
- mix_value: bfloat16 [16384, 2048], P('ep', 'tp'), may hold values from -6 to 6
- mix_gate: bfloat16 [16384, 2048], P('ep', 'tp'), may hold values from -6 to 6
- log_decay: float32 [16384, 8], P('ep', 'tp'), may hold values from -1 to 0, as said below
- ret_gain: float32 [2048], P('tp'), may hold values from 0.1 to 1.9
- w_out: bfloat16 [2048, 2048], replicated, may hold values from -0.125 to 0.125
- moe_in: bfloat16 [1024, 2048], P(('ep', 'tp')), may hold values from -6 to 6
- route_ids: int32 [1024, 2], P(('ep', 'tp')), may hold values from 0 to 7, as said below
- route_weights: float32 [1024, 2], P(('ep', 'tp')), may hold values from 0.1 to 1
- moe_gain: float32 [2048], replicated, may hold values from 0.1 to 1.9
- w_gate: bfloat16 [8, 2048, 7168], P('ep', None, 'tp'), may hold values from -0.125 to 0.125
- w_up: bfloat16 [8, 2048, 7168], P('ep', None, 'tp'), may hold values from -0.125 to 0.125
- w_down: bfloat16 [8, 7168, 2048], P('ep', 'tp'), may hold values from -0.0625 to 0.0625
Outputs:
- mix_out: bfloat16 [16384, 2048], P(('ep', 'tp'))
- moe_out: bfloat16 [1024, 2048], P(('ep', 'tp'))
Inputs may be any that keep to these rules, and one draw needn't show every extreme that they name: `log_decay`: log of a decay. `route_ids`: each row names 2 different experts. Among the rows of one device no expert is named by more than 16 rows, and one expert is named by exactly 16 rows of every device.
All inputs are finite; a program needn't handle non-finite values.
Results may differ from a plain program's by a relative error of at most 0.015.
Values may be sent and summed in bfloat16 or wider, within the bound.
A program may use at most 128 MiB of HBM per device.

v0:
```python
import jax
import jax.numpy as jnp
from jax import lax
from jax.sharding import PartitionSpec as P

HEAD_DIM = 256
BLOCK = 512


norm_eps = 1e-06


def prefix(x, axis, join, neutral):
    place = lax.axis_index(axis)
    gathered = jax.tree.map(
        lambda a, kind: lax.all_gather(a.astype(kind), axis), x, (jnp.bfloat16, jnp.bfloat16)
    )
    state = jax.tree.map(lambda a, e: jnp.zeros_like(a) + jnp.asarray(e, a.dtype), x, neutral)

    def one(hop, state):
        return join(
            state,
            jax.tree.map(
                lambda a, own: lax.dynamic_index_in_dim(a, hop, 0, False).astype(own.dtype),
                gathered,
                x,
            ),
        )

    return lax.fori_loop(0, place, one, state)


def rotate(tensor, position_index):
    head_dim = tensor.shape[-1]
    half_dim = head_dim // 2
    inverse = 10000.0 ** (-(jnp.arange(half_dim, dtype=jnp.float32) * 2.0) / head_dim)
    angle = position_index.astype(jnp.float32)[:, None] * inverse[None, :]
    cosine = jnp.cos(angle)[:, None, :]
    sine = jnp.sin(angle)[:, None, :]
    front = tensor[..., :half_dim]
    back = tensor[..., half_dim:]
    return jnp.concatenate([front * cosine - back * sine, back * cosine + front * sine], axis=-1)


def chain(earlier, later):
    return (earlier[0] * later[0], later[0][:, None, None] * earlier[1] + later[1])


def carry_block(carried, block_items):
    update, block_last = block_items
    return (jnp.exp(block_last)[:, None, None] * carried + update, carried)


def mixer_half(mix_query, mix_key, mix_value, mix_gate, log_decay, ret_gain, w_out):
    seq_rows = mix_query.shape[0]
    local_heads = mix_query.shape[1] // HEAD_DIM
    block_count = seq_rows // BLOCK
    position_index = lax.axis_index("ep") * seq_rows + jnp.arange(seq_rows, dtype=jnp.int32)
    query_rot = rotate(
        mix_query.astype(jnp.float32).reshape(seq_rows, local_heads, HEAD_DIM), position_index
    ).astype(jnp.bfloat16)
    key_rot = (
        rotate(mix_key.astype(jnp.float32).reshape(seq_rows, local_heads, HEAD_DIM), position_index)
        * HEAD_DIM ** (-0.5)
    ).astype(jnp.bfloat16)
    query_blocks = query_rot.reshape(block_count, BLOCK, local_heads, HEAD_DIM)
    key_blocks = key_rot.reshape(block_count, BLOCK, local_heads, HEAD_DIM)
    value_blocks = mix_value.reshape(block_count, BLOCK, local_heads, HEAD_DIM)
    cumulative = jnp.cumsum(log_decay.reshape(block_count, BLOCK, local_heads), axis=1)
    causal = jnp.arange(BLOCK)[:, None] >= jnp.arange(BLOCK)[None, :]
    scores = jnp.einsum(
        "nihd,njhd->nhij", query_blocks, key_blocks, preferred_element_type=jnp.float32
    )
    by_head = jnp.transpose(cumulative, (0, 2, 1))
    log_gap = by_head[:, :, :, None] - by_head[:, :, None, :]
    decay_mask = jnp.where(causal, jnp.exp(jnp.where(causal, log_gap, 0.0)), 0.0)
    weights = (scores * decay_mask).astype(jnp.bfloat16)
    within_block = jnp.einsum(
        "nhij,njhe->nihe", weights, value_blocks, preferred_element_type=jnp.float32
    )
    block_last = cumulative[:, -1, :]
    key_decayed = (
        key_blocks.astype(jnp.float32) * jnp.exp(block_last[:, None, :] - cumulative)[..., None]
    ).astype(jnp.bfloat16)
    updates = jnp.einsum(
        "njhd,njhe->nhde", key_decayed, value_blocks, preferred_element_type=jnp.float32
    )
    empty_state = jnp.zeros((local_heads, HEAD_DIM, HEAD_DIM), jnp.float32)
    local_end, starts = lax.scan(carry_block, empty_state, (updates, block_last))
    through = jnp.cumsum(block_last, axis=0)
    before = through - block_last
    incoming = prefix(
        (jnp.exp(through[-1]), local_end), "ep", chain, (jnp.ones_like(through[-1]), empty_state)
    )
    block_states = starts + jnp.exp(before)[:, :, None, None] * incoming[1][None]
    query_decayed = query_blocks.astype(jnp.float32) * jnp.exp(cumulative)[..., None]
    carried_part = jnp.einsum(
        "nihd,nhde->nihe", query_decayed, block_states, precision=lax.Precision.HIGHEST
    )
    retained = (within_block + carried_part).reshape(seq_rows, local_heads, HEAD_DIM)
    inverse_rms = lax.rsqrt(jnp.mean(retained * retained, axis=-1, keepdims=True) + norm_eps)
    gate_act = jax.nn.silu(mix_gate.astype(jnp.float32).reshape(seq_rows, local_heads, HEAD_DIM))
    heads_out = (
        gate_act * retained * inverse_rms * ret_gain.reshape(local_heads, HEAD_DIM)
    ).astype(jnp.bfloat16)
    by_rows = lax.all_to_all(
        heads_out.reshape(seq_rows, local_heads * HEAD_DIM),
        "tp",
        split_axis=0,
        concat_axis=1,
        tiled=True,
    )
    return jnp.dot(by_rows, w_out, preferred_element_type=jnp.float32).astype(jnp.bfloat16)


def expert_half(moe_in, route_ids, route_weights, moe_gain, w_gate, w_up, w_down):
    tokens, model_width = moe_in.shape
    route_count = route_ids.shape[1]
    experts = lax.axis_size("ep")
    lane_count = lax.axis_size("tp")
    capacity = 4 * tokens // experts
    floats = moe_in.astype(jnp.float32)
    normed = (
        floats * lax.rsqrt(jnp.mean(floats * floats, axis=-1, keepdims=True) + norm_eps) * moe_gain
    ).astype(jnp.bfloat16)
    flat_ids = route_ids.reshape(-1)
    onehot = (flat_ids[:, None] == jnp.arange(experts, dtype=jnp.int32)[None, :]).astype(jnp.int32)
    slot_index = jnp.sum(jnp.cumsum(onehot, axis=0) * onehot, axis=1) - 1
    target = flat_ids * capacity + slot_index
    source = jnp.arange(tokens * route_count, dtype=jnp.int32) // route_count
    slot_owner = jnp.full((experts * capacity,), tokens, jnp.int32).at[target].set(source)
    padded = jnp.concatenate([normed, jnp.zeros((1, model_width), jnp.bfloat16)], axis=0)
    outgoing = padded[slot_owner]
    gate_weight = w_gate[0]
    up_weight = w_up[0]
    down_weight = w_down[0]
    copies = jnp.broadcast_to(
        outgoing.reshape(experts, 1, capacity, model_width),
        (experts, lane_count, capacity, model_width),
    )
    arrived = lax.all_to_all(
        copies.reshape(experts * lane_count * capacity, model_width),
        ("ep", "tp"),
        split_axis=0,
        concat_axis=0,
        tiled=True,
    )
    gate_part = jnp.dot(arrived, gate_weight, preferred_element_type=jnp.float32)
    up_part = jnp.dot(arrived, up_weight, preferred_element_type=jnp.float32)
    hidden_grid = (
        (jax.nn.silu(gate_part) * up_part)
        .astype(jnp.bfloat16)
        .reshape(experts, lane_count, capacity, -1)
    )
    partial_value = jnp.einsum(
        "elcf,fd->lecd", hidden_grid, down_weight, preferred_element_type=jnp.float32
    )
    summed_rows = lax.psum_scatter(
        partial_value.reshape(lax.axis_size("tp") * (experts * capacity), model_width).astype(
            jnp.bfloat16
        ),
        "tp",
        scatter_dimension=0,
        tiled=True,
    )
    returned = lax.all_to_all(summed_rows, "ep", split_axis=0, concat_axis=0, tiled=True)
    picked_rows = returned[target].reshape(tokens, route_count, model_width)
    combined = jnp.sum(picked_rows.astype(jnp.float32) * route_weights[:, :, None], axis=1)
    return combined.astype(jnp.bfloat16)


def on_device(
    mix_query,
    mix_key,
    mix_value,
    mix_gate,
    log_decay,
    ret_gain,
    w_out,
    moe_in,
    route_ids,
    route_weights,
    moe_gain,
    w_gate,
    w_up,
    w_down,
):
    mix_out = mixer_half(mix_query, mix_key, mix_value, mix_gate, log_decay, ret_gain, w_out)
    moe_out = expert_half(moe_in, route_ids, route_weights, moe_gain, w_gate, w_up, w_down)
    return (mix_out, moe_out)


def solution(mesh):
    in_specs = (
        P("ep", "tp"),
        P("ep", "tp"),
        P("ep", "tp"),
        P("ep", "tp"),
        P("ep", "tp"),
        P("tp"),
        P(),
        P(("ep", "tp"), None),
        P(("ep", "tp"), None),
        P(("ep", "tp"), None),
        P(),
        P("ep", None, "tp"),
        P("ep", None, "tp"),
        P("ep", "tp", None),
    )
    out_specs = (P(("ep", "tp"), None), P(("ep", "tp"), None))
    return jax.shard_map(
        on_device, mesh=mesh, in_specs=in_specs, out_specs=out_specs, check_vma=False
    )
```

profile of v0, /device:TPU:0, one launch (start us, length us, event | category | flops | bytes accessed | tf_op | source)
XLA Modules:
  0.0 214.7 jit_solution(8959980904177569203)
XLA Ops:
  15.6 7.5 %all-to-all-start.1 = ((bf16[32,16,2048]{2,1,0:T(8,128)(2,1)}), bf16[32,16,2048]{2,1,0:T(8,128)(2,1)}, u32[]{:S(2)}, u32[]{:S(2)}) async-start(bf16[32,16,2048]{2,1,0:T(8,128)(2,1)} %bitcast.23), calls=%async_computation.1 | async-start | bytes 4194304 | tf_op jit(solution)/shard_map/all_to_all | solution.py:141
  26.9 2.9 %copy.165 = bf16[2048,512]{0,1:T(8,128)(2,1)S(1)} copy(bf16[2048,512]{1,0:T(8,128)(2,1)} %param.18) | data formatting | bytes 4194304 | tf_op args[0]
  29.8 2.5 %convert.15 = f32[2048,2,256]{0,2,1:T(8,128)} convert(bf16[2048,2,256]{0,2,1:T(8,128)(2,1)S(1)} %bitcast.104) | non-fusion elementwise | flops 1048576 | bytes 6291456 | tf_op jit(solution)/shard_map/reshape | solution.py:60
  32.3 2.9 %copy.170 = bf16[2048,512]{0,1:T(8,128)(2,1)S(1)} copy(bf16[2048,512]{1,0:T(8,128)(2,1)} %param.19) | data formatting | bytes 4194304 | tf_op args[1]
  35.7 3.7 %multiply_cosine_fusion = (f32[2048,128]{0,1:T(8,128)S(1)}, f32[2048,128]{0,1:T(8,128)S(1)}) fusion(f32[128]{0:T(128)S(1)} %multiply_power_fusion, f32[2048]{0:T(1024)S(1)} %add_convert_fusion.1), kind=kLoop, calls=%fused_computation.61 | loop fusion | flops 262144 | bytes 2105856 | tf_op jit(solution)/shard_map/cos | solution.py:38
  39.5 3.1 %multiply_subtract_fusion = (f32[2048,2,128]{0,2,1:T(8,128)}, f32[2048,2,128]{0,2,1:T(8,128)S(1)}, bf16[2048,2,128]{0,2,1:T(8,128)(2,1)S(1)}, bf16[2048,2,128]{0,2,1:T(8,128)(2,1)}) fusion(f32[2048,2,256]{0,2,1:T(8,128)S(1)} %convert.16, f32[2048,128]{0,1:T(8,128)S(1)} %get-tuple-element.194, f32[2048,128]{0,1:T(8,128)S(1)} %get-tuple-element.193, ...), kind=kLoop, calls=%fused_computation.53 | loop fusion | flops 7340032 | bytes 16777216 | tf_op jit(solution)/shard_map/sub | solution.py:42
  42.5 2.9 %copy.171 = f32[2048,2,128]{2,0,1:T(8,128)} copy(f32[2048,2,128]{0,2,1:T(8,128)} %get-tuple-element.185) | data formatting | bytes 4194304 | tf_op jit(solution)/shard_map/sub | solution.py:42
  47.3 4.2 %reshape.244 = bf16[4,512,2,256]{3,2,1,0:T(2,128)(2,1)} reshape(bf16[2048,512]{1,0:T(8,128)(2,1)} %param.20) | data formatting | bytes 4194304 | tf_op jit(solution)/shard_map/reshape | solution.py:68
  51.4 5.1 %fusion.36 = f32[4,2,256,256]{3,2,1,0:T(8,128)} fusion(f32[4,512,2]{1,2,0:T(2,128)S(1)} %copy.180, bf16[4,512,2,256]{3,2,1,0:T(2,128)(2,1)} %reshape.244, f32[4,512,2,128]{3,1,0,2:T(8,128)} %bitcast.115, f32[4,512,2,128]{3,1,0,2:T(8,128)S(1)} %bitcast.114), kind=kOutput, calls=%fused_computation.46 | convolution fusion | flops 543162368 | bytes 8404992 | tf_op jit(solution)/shard_map/njhd,njhe->nhde/dot_general | solution.py:85
  56.6 8.1 %while.26 = (s32[]{:T(128)}, f32[2,256,256]{2,1,0:T(8,128)S(1)}, f32[4,2,256,256]{3,2,1,0:T(8,128)}, f32[4,2]{1,0:T(4,128)S(1)}, f32[4,2,256,256]{3,2,1,0:T(8,128)}, /*index=5*/s32[]{:T(128)}, s32[]{:T(128)}) while((s32[]{:T(128)}, f32[2,256,256]{2,1,0:T(8,128)S(1)}, f32[4,2,256,256]{3,2,1,0:T(8,128)}, f32[4,2]{1,0:T(4,128)S(1)}, ...), condition=%wide.region_3.4_spmd.clone, body=%wide.region_2.3_spmd.clone.sunk | while | flops 524291 | bytes 2622072 | solution.py:89
  65.9 20.9 %all-gather.1 = bf16[8,1,2]{2,1,0:T(2,128)(2,1)S(1)} all-gather(bf16[1,1,2]{2,1,0:T(2,128)(2,1)S(1)} %bitcast.125), channel_id=1, replica_groups=mesh['ep'=8,'tp'=4] {'ep'}, dimensions={0}, use_global_device_ids=true | all-gather | bytes 36 | tf_op jit(solution)/shard_map/all_gather | solution.py:16
  88.4 7.5 %fusion.14 = f32[4,2,512,256]{2,3,1,0:T(8,128)} fusion(f32[4,2,512]{2,1,0:T(2,128)S(1)} %reshape.284, pred[512,512]{1,0:T(8,128)(4,1)S(1)} %iota_compare_fusion, bf16[4,512,2,256]{3,2,1,0:T(2,128)(2,1)} %reshape.244, f32[4,512,2,128]{3,1,0,2:T(8,128)} %bitcast.116, f32[4,512,2,128]{3,1,0,2:T(8,128)} %bitcast.113, ...), kind=kOutput, calls=%fused_computation.26 | convolution fusion | flops 2165309440 | bytes 12861440 | tf_op jit(solution)/shard_map/nhij,njhe->nihe/dot_general | solution.py:78
  95.9 7.8 %fusion.6 = f32[512,1792]{1,0:T(8,128)S(1)} fusion(bf16[512,2048]{1,0:T(8,128)(2,1)} %bitcast.24, bf16[1,2048,1792]{2,1,0:T(8,128)(2,1)} %param.29), kind=kOutput, calls=%fused_computation.16 | convolution fusion | flops 3758096384 | bytes 13107200 | tf_op jit(solution)/shard_map/dot_general | solution.py:148
  103.8 8.0 %multiply_convert_fusion.3 = bf16[512,1792]{1,0:T(8,128)(2,1)S(1)} fusion(f32[512,1792]{1,0:T(8,128)S(1)} %fusion.6, bf16[512,2048]{1,0:T(8,128)(2,1)} %bitcast.24, bf16[1,2048,1792]{2,1,0:T(8,128)(2,1)} %param.30), kind=kOutput, calls=%fused_computation.41 | convolution fusion | flops 3763601408 | bytes 14942208 | tf_op jit(solution)/shard_map/dot_general | solution.py:149
  111.9 4.2 %fusion.31 = bf16[4,8,16,2048]{3,2,0,1:T(8,128)(2,1)S(1)} fusion(bf16[8,4,16,1792]{3,2,1,0:T(8,128)(2,1)S(1)} %bitcast.128, bf16[1,1792,2048]{2,1,0:T(8,128)(2,1)S(1)} %bitcast.127), kind=kOutput, calls=%fused_computation.45 | convolution fusion | flops 3759144960 | bytes 11272192 | tf_op jit(solution)/shard_map/elcf,fd->lecd/dot_general | solution.py:155
  118.0 11.4 %multiply_reduce_fusion = (f32[4,512,2]{1,2,0:T(2,128)S(1)}, f32[4,512,2,256]{1,3,2,0:T(8,128)}) fusion(f32[4,512,2]{1,2,0:T(2,128)S(1)} %copy.187, f32[4,2,256,256]{3,2,1,0:T(8,128)} %get-tuple-element.74, f32[2,256,256]{2,1,0:T(8,128)S(1)} %get-tuple-element.76, f32[4,2]{1,0:T(4,128)S(1)} %copy.184, f32[4,2,512,256]{2,3,1,0:T(8,128)} %fusion.14, ...), kind=kOutput, calls=%fused_computation.31 | convolution fusion | flops 3231707136 | bytes 13140000 | tf_op jit(solution)/shard_map/nihd,nhde->nihe/dot_general | solution.py:97
  129.8 2.5 %mul.264 = f32[2048,2,256]{2,1,0:T(2,128)S(1)} broadcast(f32[2048,2]{1,0:T(8,128)S(1)} %copy.190), dimensions={0,1} | broadcast | bytes 4210688 | tf_op jit(solution)/shard_map/mul | solution.py:104
  134.7 7.3 %copy.189 = f32[4,512,2,256]{3,2,1,0:T(2,128)} copy(f32[4,512,2,256]{1,3,2,0:T(8,128)} %get-tuple-element.196) | data formatting | bytes 8388608 | tf_op jit(solution)/shard_map/add | solution.py:100
  142.0 2.8 %copy.204 = f32[256,8,2,256]{3,1,2,0:T(8,128)S(1)} copy(f32[256,8,2,256]{3,2,1,0:T(2,128)} %bitcast.102) | data formatting | bytes 8388608
  150.2 3.7 %all-to-all-start = ((bf16[4,512,512]{1,2,0:T(8,128)(2,1)}), bf16[4,512,512]{1,2,0:T(8,128)(2,1)S(1)}, u32[]{:S(2)}, u32[]{:S(2)}) async-start(bf16[4,512,512]{1,2,0:T(8,128)(2,1)} %copy.191), calls=%async_computation | async-start | bytes 4194304 | tf_op jit(solution)/shard_map/all_to_all | solution.py:106
  154.0 25.5 %all-to-all-done = bf16[4,512,512]{1,2,0:T(8,128)(2,1)S(1)} async-done(((bf16[4,512,512]{1,2,0:T(8,128)(2,1)}), bf16[4,512,512]{1,2,0:T(8,128)(2,1)S(1)}, u32[]{:S(2)}, u32[]{:S(2)}) %all-to-all-start) | async-done | bytes 2097184 | tf_op jit(solution)/shard_map/all_to_all | solution.py:106
  179.5 11.0 %all-to-all-start.2 = ((bf16[8,16,2048]{2,1,0:T(8,128)(2,1)}), bf16[8,16,2048]{2,1,0:T(8,128)(2,1)S(1)}, u32[]{:S(2)}, u32[]{:S(2)}) async-start(bf16[8,16,2048]{2,1,0:T(8,128)(2,1)} %bitcast.119), calls=%async_computation.3 | async-start | bytes 1048576 | tf_op jit(solution)/shard_map/all_to_all | solution.py:166
  190.5 9.1 %convolution_convert_fusion = bf16[512,2048]{1,0:T(8,128)(2,1)} fusion(bf16[512,2048]{0,1:T(8,128)(2,1)S(1)} %bitcast.117, bf16[2048,2048]{1,0:T(8,128)(2,1)} %param.24), kind=kOutput, calls=%fused_computation.43 | convolution fusion | flops 4296015872 | bytes 12582912 | tf_op jit(solution)/shard_map/dot_general | solution.py:113
  199.7 5.1 %all-to-all-done.2 = bf16[8,16,2048]{2,1,0:T(8,128)(2,1)S(1)} async-done(((bf16[8,16,2048]{2,1,0:T(8,128)(2,1)}), bf16[8,16,2048]{2,1,0:T(8,128)(2,1)S(1)}, u32[]{:S(2)}, u32[]{:S(2)}) %all-to-all-start.2) | async-done | bytes 524320 | tf_op jit(solution)/shard_map/all_to_all | solution.py:166
  (101 shorter events, 37.2 us)
Async XLA Ops:
  15.6 7.5 %copy-start.5 = (f32[2048,2]{0,1:T(2,128)S(1)}, f32[2048,2]{0,1:T(2,128)}, u32[]{:S(2)}) copy-start(f32[2048,2]{0,1:T(2,128)} %param.22) | copy-start | bytes 49156
  15.6 80.4 %all-to-all-start.1 = ((bf16[32,16,2048]{2,1,0:T(8,128)(2,1)}), bf16[32,16,2048]{2,1,0:T(8,128)(2,1)}, u32[]{:S(2)}, u32[]{:S(2)}) async-start(bf16[32,16,2048]{2,1,0:T(8,128)(2,1)} %bitcast.23), calls=%async_computation.1 | async-start | bytes 4194304 | tf_op jit(solution)/shard_map/all_to_all | solution.py:141
  23.0 94.6 %all-gather.4.cloned.1.call-start = ((), (), s32[]{:S(2)}) async-start(), calls=%async_computation.5 | async-start | bytes 2359296 | tf_op jit(solution)/shard_map/all_gather | solution.py:16
  35.2 4.2 %copy-start.1 = (f32[2048,2,256]{0,2,1:T(8,128)S(1)}, f32[2048,2,256]{0,2,1:T(8,128)}, u32[]{:S(2)}) copy-start(f32[2048,2,256]{0,2,1:T(8,128)} %convert.15) | copy-start | bytes 12582916
  47.3 4.2 %copy-start.3 = (f32[2048,2,128]{2,0,1:T(8,128)S(1)}, f32[2048,2,128]{2,0,1:T(8,128)}, u32[]{:S(2)}) copy-start(f32[2048,2,128]{2,0,1:T(8,128)} %copy.171) | copy-start | bytes 6291460
  56.6 30.3 %copy-start.2 = (bf16[2048,2,128]{0,2,1:T(8,128)(2,1)S(1)}, bf16[2048,2,128]{0,2,1:T(8,128)(2,1)}, u32[]{:S(2)}) copy-start(bf16[2048,2,128]{0,2,1:T(8,128)(2,1)} %get-tuple-element.190) | copy-start | bytes 3145732
  65.4 114.1 %reduce-scatter.2.cloned.1.call-start = ((), (), s32[]{:S(2)}) async-start(), calls=%async_computation.4 | async-start | bytes 2621440 | tf_op jit(solution)/shard_map/reduce_scatter | solution.py:158
  95.9 15.9 %slice-start = ((s8[7340032]{0:T(1024)(128)(4,1)}), s8[4194304]{0:T(1024)(128)(4,1)S(1)}, s32[]{:S(2)}) async-start(s8[7340032]{0:T(1024)(128)(4,1)} %bitcast.126), calls=%async_computation.6 | async-start | bytes 8388608
  103.8 8.1 %slice-start.1 = ((s8[7340032]{0:T(1024)(128)(4,1)}), s8[3145728]{0:T(1024)(128)(4,1)S(1)}, s32[]{:S(2)}) async-start(s8[7340032]{0:T(1024)(128)(4,1)} %bitcast.126), calls=%async_computation.7 | async-start | bytes 6291456
  142.0 3.5 %copy-start = (f32[256,8,2,256]{3,1,2,0:T(8,128)S(1)}, f32[256,8,2,256]{3,1,2,0:T(8,128)}, u32[]{:S(2)}) copy-start(f32[256,8,2,256]{3,1,2,0:T(8,128)} %copy.205) | copy-start | bytes 12582916
  142.0 4.2 %copy-start.4 = (bf16[2048,512]{1,0:T(8,128)(2,1)S(1)}, bf16[2048,512]{1,0:T(8,128)(2,1)}, u32[]{:S(2)}) copy-start(bf16[2048,512]{1,0:T(8,128)(2,1)} %param.21) | copy-start | bytes 6291460
  142.0 4.2 %copy-start.6 = (f32[512]{0:T(512)S(1)}, f32[512]{0:T(512)}, u32[]{:S(2)}) copy-start(f32[512]{0:T(512)} %param.23) | copy-start | bytes 6148
  150.2 3.8 %copy-start.7 = (f32[32,2]{0,1:T(2,128)S(1)}, f32[32,2]{0,1:T(2,128)}, u32[]{:S(2)}) copy-start(f32[32,2]{0,1:T(2,128)} %param.27) | copy-start | bytes 772
  150.2 29.4 %all-to-all-start = ((bf16[4,512,512]{1,2,0:T(8,128)(2,1)}), bf16[4,512,512]{1,2,0:T(8,128)(2,1)S(1)}, u32[]{:S(2)}, u32[]{:S(2)}) async-start(bf16[4,512,512]{1,2,0:T(8,128)(2,1)} %copy.191), calls=%async_computation | async-start | bytes 4194304 | tf_op jit(solution)/shard_map/all_to_all | solution.py:106
  179.5 25.2 %all-to-all-start.2 = ((bf16[8,16,2048]{2,1,0:T(8,128)(2,1)}), bf16[8,16,2048]{2,1,0:T(8,128)(2,1)S(1)}, u32[]{:S(2)}, u32[]{:S(2)}) async-start(bf16[8,16,2048]{2,1,0:T(8,128)(2,1)} %bitcast.119), calls=%async_computation.3 | async-start | bytes 1048576 | tf_op jit(solution)/shard_map/all_to_all | solution.py:166
Sparse Core Ops, SparseCore 0:
  65.6 50.4 all-gather.3
Sparse Core Ops, SparseCore 1:
  117.7 28.5 reduce-scatter.1
where the time goes:
time: 216 us; the launch traced here: 215 us
  matrix products  53.2 us (25%)
  local copies, waits for them, and re-layouts  43.1 us (20%)
  waiting for transfers between devices  30.7 us (14%)
  other arithmetic  28.4 us (13%)
  starting transfers between devices  22.3 us (10%)
  blocking collectives  20.9 us (10%)
  between operations  15.9 us (7%)
    all_to_all x1, waiting for transfers between devices, mixer_half(): lax.all_to_all(heads_out.reshape(seq_rows, local_heads * HEAD_DIM), 'tp',...  25.5 us
    all_gather x1, blocking collectives, prefix(): lax.all_gather(a.astype(kind), axis)  20.9 us
    unnamed x27, local copies, waits for them, and re-layouts  13.4 us
    dot_general x1, matrix products, mixer_half(): jnp.einsum('nihd,nhde->nihe', query_decayed, block_states, precision=lax....  11.4 us
    all_to_all x1, starting transfers between devices, expert_half(): lax.all_to_all(summed_rows, 'ep', split_axis=0, concat_axis=0, tiled=True)  11 us
    dot_general x1, matrix products, mixer_half(): jnp.dot(by_rows, w_out, preferred_element_type=jnp.float32)  9.11 us
    dot_general x1, matrix products, expert_half(): up_part = jnp.dot(arrived, up_weight, preferred_element_type=jnp.float32)  8.03 us
    dot_general x1, matrix products, expert_half(): jnp.dot(arrived, gate_weight, preferred_element_type=jnp.float32)  7.83 us
  transfers between devices with their start and end apart: 5, of which 2 were waited for; matrix products, arithmetic and copies ran while one was open for 53% of the time, Pallas kernels for 0%

commit v1 on v0

v1 whole, which is shorter than its diff:
```python
import functools

import jax
import jax.numpy as jnp
import numpy as np
from jax import lax
from jax.experimental import pallas as pl
from jax.experimental.pallas import tpu as pltpu
from jax.sharding import PartitionSpec as P

HEAD_DIM = 256
BLOCK = 512
norm_eps = 1e-06
F32 = jnp.float32
BF16 = jnp.bfloat16
VMEM_LIMIT = 60 * 1024 * 1024
TAIL = 16


def params(*semantics):
    return pltpu.CompilerParams(
        dimension_semantics=semantics or None, vmem_limit_bytes=VMEM_LIMIT
    )


def cost(flops, moved, exps=0):
    return pl.CostEstimate(flops=int(flops), bytes_accessed=int(moved), transcendentals=int(exps))


def dot(a, b, ca=1, cb=0):
    return lax.dot_general(a, b, (((ca,), (cb,)), ((), ())), preferred_element_type=F32)


def split3(x):
    a = x.astype(BF16)
    rest = x - a.astype(F32)
    b = rest.astype(BF16)
    c = (rest - b.astype(F32)).astype(BF16)
    return a, b, c


def retention_kernel(
    slices, place_ref, q_ref, k_ref, v_ref, l_ref, cos_r, sin_r, cos_b, sin_b,
    local_ref, qd_ref, message_ref, state, before,
):
    head = pl.program_id(0)
    block = pl.program_id(1)
    size = q_ref.shape[0]
    half = HEAD_DIM // 2

    @pl.when(block == 0)
    def _():
        state[...] = jnp.zeros_like(state)
        before[...] = jnp.zeros_like(before)

    rows = lax.broadcasted_iota(jnp.int32, (size, size), 0)
    cols = lax.broadcasted_iota(jnp.int32, (size, size), 1)
    upper = jnp.where(rows <= cols, 1.0, 0.0).astype(BF16)
    a, b, c = split3(l_ref[...])
    sums = dot(a, upper) + dot(b, upper) + dot(c, upper)
    pick = lax.broadcasted_iota(jnp.int32, sums.shape, 0) == head
    cum_row = jnp.sum(jnp.where(pick, sums, 0.0), axis=0, keepdims=True)
    cum_col = jnp.transpose(jnp.broadcast_to(cum_row, (8, size)))[:, 0:1]
    last = cum_row[:, size - 1 : size]

    cb, sb = cos_b[0], sin_b[0]
    cosine = cos_r[...] * cb - sin_r[...] * sb
    sine = sin_r[...] * cb + cos_r[...] * sb

    def rotate(x):
        front = x[:, :half].astype(F32)
        back = x[:, half:].astype(F32)
        return jnp.concatenate(
            [front * cosine - back * sine, back * cosine + front * sine], axis=1
        )

    q_rot = rotate(q_ref[...]).astype(BF16)
    k_rot = (rotate(k_ref[...]) * HEAD_DIM ** (-0.5)).astype(BF16)
    value = v_ref[...]
    q_wide = q_rot.astype(F32)
    grown = before[0:1, 0:1]
    decay_in = jnp.exp(cum_col)
    q_decayed = (q_wide * decay_in).astype(BF16)
    qd_ref[...] = (q_wide * jnp.exp(cum_col + grown)).astype(BF16)
    old = state[...]
    carried = dot(q_decayed, old.astype(BF16))
    step = size // 2
    for i in range(2):
        r0, width = i * step, (i + 1) * step
        scores = dot(q_rot[r0 : r0 + step], k_rot[:width], 1, 1)
        causal = (
            lax.broadcasted_iota(jnp.int32, (step, width), 0) + r0
            >= lax.broadcasted_iota(jnp.int32, (step, width), 1)
        )
        gap = cum_col[r0 : r0 + step] - cum_row[:, :width]
        mask = jnp.exp(jnp.where(causal, gap, -1e30))
        weights = (scores * mask).astype(BF16)
        local_ref[r0 : r0 + step, :] = dot(weights, value[:width]) + carried[r0 : r0 + step]
    k_decayed = (k_rot.astype(F32) * jnp.exp(last - cum_col)).astype(BF16)
    fresh = jnp.exp(last) * old + dot(k_decayed, value, 0, 0)
    state[...] = fresh
    before[...] = before[...] + last

    @pl.when(block == pl.num_programs(1) - 1)
    def _():
        part = HEAD_DIM // slices
        total = jnp.exp(before[0:1, 0:1])
        tail = jnp.broadcast_to(total, (TAIL, HEAD_DIM)).astype(BF16)
        for i in range(slices):
            message_ref[i, :part, :] = fresh[i * part : (i + 1) * part].astype(BF16)
            message_ref[i, part:, :] = tail


def retention(mix_query, mix_key, mix_value, log_decay, devices, place):
    rows, width = mix_query.shape
    heads = width // HEAD_DIM
    blocks = rows // BLOCK
    half = HEAD_DIM // 2
    slices = devices // heads
    part = HEAD_DIM // slices
    inverse = 10000.0 ** (-(np.arange(half) * 2.0) / HEAD_DIM)
    fine = np.arange(BLOCK)[:, None] * inverse[None, :]
    coarse = (np.arange(devices * blocks) * BLOCK)[:, None, None] * inverse[None, None, :]
    tables = [np.asarray(f(x), np.float32) for x in (fine, coarse) for f in (np.cos, np.sin)]
    logs = jnp.pad(log_decay.T, ((0, 8 - heads), (0, 0)))
    tile = pl.BlockSpec((BLOCK, HEAD_DIM), lambda h, b, p: (b, h))
    whole = pl.BlockSpec((BLOCK, half), lambda h, b, p: (0, 0))
    base = pl.BlockSpec((1, 1, half), lambda h, b, p: (p[0] * blocks + b, 0, 0))
    return pl.pallas_call(
        functools.partial(retention_kernel, slices),
        grid_spec=pltpu.PrefetchScalarGridSpec(
            num_scalar_prefetch=1,
            grid=(heads, blocks),
            in_specs=[
                tile, tile, tile,
                pl.BlockSpec((8, BLOCK), lambda h, b, p: (0, b)),
                whole, whole, base, base,
            ],
            out_specs=[
                tile, tile,
                pl.BlockSpec((slices, part + TAIL, HEAD_DIM), lambda h, b, p: (h, 0, 0)),
            ],
            scratch_shapes=[pltpu.VMEM((HEAD_DIM, HEAD_DIM), F32), pltpu.VMEM((8, 128), F32)],
        ),
        out_shape=[
            jax.ShapeDtypeStruct((rows, width), F32),
            jax.ShapeDtypeStruct((rows, width), BF16),
            jax.ShapeDtypeStruct((devices, part + TAIL, HEAD_DIM), BF16),
        ],
        compiler_params=params("arbitrary", "arbitrary"),
        cost_estimate=cost(rows * width * (4 * BLOCK + 4 * HEAD_DIM) * 2, rows * width * 12),
        name="retention",
    )(place, mix_query, mix_key, mix_value, logs, tables[0], tables[1], tables[2], tables[3])


def prefix_kernel(in_ref, out_ref):
    part = out_ref.shape[1]
    state = jnp.zeros(out_ref.shape[1:], F32)
    for s in range(out_ref.shape[0]):
        out_ref[s] = state.astype(BF16)
        state = in_ref[s, part : part + 1, :].astype(F32) * state + in_ref[s, :part, :].astype(F32)


def prefix(messages):
    devices, length, width = messages.shape
    return pl.pallas_call(
        prefix_kernel,
        out_shape=jax.ShapeDtypeStruct((devices, length - TAIL, width), BF16),
        compiler_params=params(),
        cost_estimate=cost(messages.size * 2, messages.size * 4),
        name="prefix",
    )(messages)


def finish_kernel(local_ref, qd_ref, in_ref, gate_ref, gain_ref, out_ref):
    retained = local_ref[...] + dot(qd_ref[...], in_ref[0])
    inverse_rms = lax.rsqrt(jnp.mean(retained * retained, axis=-1, keepdims=True) + norm_eps)
    gate = gate_ref[...].astype(F32)
    gate = gate / (1.0 + jnp.exp(-gate))
    out_ref[...] = (gate * retained * inverse_rms * gain_ref[...]).astype(BF16)


def finish(head, local, q_decayed, incoming, mix_gate, ret_gain):
    rows = local.shape[0]
    tile = pl.BlockSpec((BLOCK, HEAD_DIM), lambda b: (b, head))
    return pl.pallas_call(
        finish_kernel,
        grid=(rows // BLOCK,),
        in_specs=[
            tile, tile,
            pl.BlockSpec((1, HEAD_DIM, HEAD_DIM), lambda b: (head, 0, 0)),
            tile,
            pl.BlockSpec((1, HEAD_DIM), lambda b: (0, head)),
        ],
        out_specs=pl.BlockSpec((BLOCK, HEAD_DIM), lambda b: (b, 0)),
        out_shape=jax.ShapeDtypeStruct((rows, HEAD_DIM), BF16),
        compiler_params=params("arbitrary"),
        cost_estimate=cost(rows * HEAD_DIM * HEAD_DIM * 2, rows * HEAD_DIM * 10),
        name="finish",
    )(local, q_decayed, incoming, mix_gate, ret_gain)


def project_kernel(lanes, heads, *refs):
    pieces, w_ref, out_ref = refs[:heads], refs[heads], refs[heads + 1]
    total = None
    for h in range(heads):
        for lane in range(lanes):
            r0 = (lane * heads + h) * HEAD_DIM
            term = dot(pieces[h][lane], w_ref[r0 : r0 + HEAD_DIM, :])
            total = term if total is None else total + term
    out_ref[...] = total.astype(BF16)


def project(pieces, w_out):
    heads = len(pieces)
    lanes, rows, _ = pieces[0].shape
    depth, width = w_out.shape
    tile = 256
    return pl.pallas_call(
        functools.partial(project_kernel, lanes, heads),
        grid=(width // tile,),
        in_specs=[pl.BlockSpec((lanes, rows, HEAD_DIM), lambda n: (0, 0, 0))] * heads
        + [pl.BlockSpec((depth, tile), lambda n: (0, n))],
        out_specs=pl.BlockSpec((rows, tile), lambda n: (0, n)),
        out_shape=jax.ShapeDtypeStruct((rows, width), BF16),
        compiler_params=params("arbitrary"),
        cost_estimate=cost(2 * rows * depth * width, 2 * (rows * depth + depth * width)),
        name="project",
    )(*pieces, w_out)


def slots_of(ids, capacity, count):
    tokens = ids.shape[0]
    lane = lax.broadcasted_iota(jnp.int32, (tokens, count), 1)
    expert = lane // capacity
    first = ids[:, 0:1] == expert
    second = ids[:, 1:2] == expert
    member = jnp.where(first | second, 1.0, 0.0)
    earlier = jnp.where(
        lax.broadcasted_iota(jnp.int32, (tokens, tokens), 0)
        > lax.broadcasted_iota(jnp.int32, (tokens, tokens), 1),
        1.0,
        0.0,
    ).astype(BF16)
    taken = dot(earlier, member.astype(BF16))
    slot = (lane - expert * capacity).astype(F32)
    return jnp.where(taken == slot, member, 0.0), first


def dispatch_kernel(capacity, x_ref, ids_ref, gain_ref, out_ref):
    floats = x_ref[...].astype(F32)
    scale = lax.rsqrt(jnp.mean(floats * floats, axis=-1, keepdims=True) + norm_eps)
    normed = (floats * scale * gain_ref[...]).astype(BF16)
    chosen, _ = slots_of(ids_ref[...], capacity, out_ref.shape[0])
    out_ref[...] = dot(chosen.astype(BF16), normed, 0, 0).astype(BF16)


def dispatch(moe_in, route_ids, moe_gain, experts, capacity):
    width = moe_in.shape[1]
    return pl.pallas_call(
        functools.partial(dispatch_kernel, capacity),
        out_shape=jax.ShapeDtypeStruct((experts * capacity, width), BF16),
        compiler_params=params(),
        cost_estimate=cost(moe_in.size * 256, moe_in.size * 8),
        name="dispatch",
    )(moe_in, route_ids, moe_gain.reshape(1, width))


def combine_kernel(capacity, x_ref, ids_ref, w_ref, out_ref):
    chosen, first = slots_of(ids_ref[...], capacity, x_ref.shape[0])
    weight = chosen * jnp.where(first, w_ref[:, 0:1], w_ref[:, 1:2])
    x = x_ref[...]
    total = None
    for term in split3(weight):
        part = dot(term, x)
        total = part if total is None else total + part
    out_ref[...] = total.astype(BF16)


def combine(returned, route_ids, route_weights, capacity):
    tokens = route_ids.shape[0]
    return pl.pallas_call(
        functools.partial(combine_kernel, capacity),
        out_shape=jax.ShapeDtypeStruct((tokens, returned.shape[1]), BF16),
        compiler_params=params(),
        cost_estimate=cost(returned.size * 200, returned.size * 4),
        name="combine",
    )(returned, route_ids, route_weights)


def up_kernel(count, *refs):
    pieces, g_ref, u_ref, out_ref, x = refs[:count], *refs[count:]
    rows = pieces[0].shape[0]

    @pl.when(pl.program_id(0) == 0)
    def _():
        for i in range(count):
            x[i * rows : (i + 1) * rows, :] = pieces[i][...]

    gate = dot(x[...], g_ref[0])
    up = dot(x[...], u_ref[0])
    out_ref[...] = (gate / (1.0 + jnp.exp(-gate)) * up).astype(BF16)


def expert_up(pieces, w_gate, w_up):
    count = len(pieces)
    rows, depth = pieces[0].shape
    width = w_gate.shape[2]
    tile = 256 if width % 256 == 0 else 128
    weight = pl.BlockSpec((1, depth, tile), lambda n: (0, 0, n))
    total = rows * count
    return pl.pallas_call(
        functools.partial(up_kernel, count),
        grid=(width // tile,),
        in_specs=[pl.BlockSpec((rows, depth), lambda n: (0, 0))] * count + [weight, weight],
        out_specs=pl.BlockSpec((total, tile), lambda n: (0, n)),
        out_shape=jax.ShapeDtypeStruct((total, width), BF16),
        scratch_shapes=[pltpu.VMEM((total, depth), BF16)],
        compiler_params=params("arbitrary"),
        cost_estimate=cost(4 * total * depth * width, 4 * depth * width),
        name="expert_up",
    )(*pieces, w_gate, w_up)


def down_kernel(h_ref, w_ref, keep_ref, send_ref):
    y = dot(h_ref[...], w_ref[0]).astype(BF16)
    rows = keep_ref.shape[0]
    keep_ref[...] = y[:rows]
    send_ref[...] = y[rows:]


def expert_down(hidden, w_down):
    rows, depth = hidden.shape
    width = w_down.shape[2]
    tile = 256
    out = pl.BlockSpec((rows // 2, tile), lambda n: (0, n))
    return pl.pallas_call(
        down_kernel,
        grid=(width // tile,),
        in_specs=[
            pl.BlockSpec((rows, depth), lambda n: (0, 0)),
            pl.BlockSpec((1, depth, tile), lambda n: (0, 0, n)),
        ],
        out_specs=[out, out],
        out_shape=[jax.ShapeDtypeStruct((rows // 2, width), BF16)] * 2,
        compiler_params=params("arbitrary"),
        cost_estimate=cost(2 * rows * depth * width, 2 * depth * width),
        name="expert_down",
    )(hidden, w_down)


def exchange(x, axis):
    return lax.all_to_all(x, axis, split_axis=0, concat_axis=0, tiled=True)


def to_core(x, lanes):
    return lax.ppermute(x, "tp", [(i, i ^ 1) for i in range(lanes)])


def to_chip(x, shift, lanes):
    return lax.ppermute(x, "tp", [(i, (i + 2 * shift) % lanes) for i in range(lanes)])


def on_device(
    mix_query, mix_key, mix_value, mix_gate, log_decay, ret_gain, w_out,
    moe_in, route_ids, route_weights, moe_gain, w_gate, w_up, w_down,
):
    devices = lax.axis_size("ep")
    lanes = lax.axis_size("tp")
    chips = lanes // 2
    place = lax.axis_index("ep").astype(jnp.int32).reshape(1)
    heads = mix_query.shape[1] // HEAD_DIM
    tokens, model_width = moe_in.shape
    capacity = 4 * tokens // devices

    outgoing = dispatch(moe_in, route_ids, moe_gain, devices, capacity)
    own = exchange(outgoing, "ep")

    local, q_decayed, message = retention(
        mix_query, mix_key, mix_value, log_decay, devices, place
    )
    incoming = exchange(prefix(exchange(message, "ep")), "ep")
    incoming = incoming.reshape(heads, HEAD_DIM, HEAD_DIM)

    near = [own] + [to_chip(own, s, lanes) for s in range(1, chips)]
    pieces = near + [to_core(x, lanes) for x in near]

    gain = ret_gain.reshape(1, -1)
    gathered = []
    for h in range(heads):
        out = finish(h, local, q_decayed, incoming, mix_gate, gain)
        gathered.append(exchange(out.reshape(lanes, -1, HEAD_DIM), "tp"))

    hidden = expert_up(pieces, w_gate, w_up)
    keep, send = expert_down(hidden, w_down)
    joined = (keep.astype(F32) + to_core(send, lanes).astype(F32)).astype(BF16)
    joined = joined.reshape(chips, -1, model_width)
    total = joined[0].astype(F32)
    for s in range(1, chips):
        total = total + to_chip(joined[s], -s, lanes).astype(F32)
    returned = exchange(total.astype(BF16), "ep")
    moe_out = combine(returned, route_ids, route_weights, capacity)
    mix_out = project(gathered, w_out)
    return (mix_out, moe_out)


def solution(mesh):
    in_specs = (
        P("ep", "tp"),
        P("ep", "tp"),
        P("ep", "tp"),
        P("ep", "tp"),
        P("ep", "tp"),
        P("tp"),
        P(),
        P(("ep", "tp"), None),
        P(("ep", "tp"), None),
        P(("ep", "tp"), None),
        P(),
        P("ep", None, "tp"),
        P("ep", None, "tp"),
        P("ep", "tp", None),
    )
    out_specs = (P(("ep", "tp"), None), P(("ep", "tp"), None))
    return jax.shard_map(
        on_device, mesh=mesh, in_specs=in_specs, out_specs=out_specs, check_vma=False
    )
```

time: 216 us -> 169 us (0.78)
  Pallas kernels: 0 us -> 63.6 us
  matrix products: 53.2 us -> 0 us
  local copies, waits for them, and re-layouts: 43.1 us -> 6.61 us
  other arithmetic: 28.4 us -> 1.33 us
  blocking collectives: 20.9 us -> 37.4 us
  between operations: 15.9 us -> 0.73 us
  waiting for transfers between devices: 30.7 us -> 37.9 us
  starting transfers between devices: 22.3 us -> 19.6 us
    pallas_call x0 -> x9, Pallas kernels: none -> 63.6 us  [the longest x1 14.6 us: retention(): pl.pallas_call(functools.partial(retention_kernel, slices), grid_spec=plt...]
    dot_general x7 -> x0, matrix products: 53.2 us -> none  [the longest x1 11.4 us: mixer_half(): jnp.einsum('nihd,nhde->nihe', query_decayed, block_states, precision=lax....]
    all_to_all x0 -> x2, blocking collectives: none -> 37.4 us  [exchange(): return lax.all_to_all(x, axis, split_axis=0, concat_axis=0, tiled=True)]
    all_gather x1 -> x0, blocking collectives: 20.9 us -> none  [prefix(): lax.all_gather(a.astype(kind), axis)]
    ppermute x0 -> x5, waiting for transfers between devices: none -> 17.1 us  [the longest x2 17.1 us: to_chip(): lax.ppermute(x, 'tp', [(i, (i + 2 * shift) % lanes) for i in range(lanes)])]
    all_to_all x3 -> x4, waiting for transfers between devices: 30.7 us -> 20.8 us  [exchange(): return lax.all_to_all(x, axis, split_axis=0, concat_axis=0, tiled=True)]
    add x2 -> x0, local copies, waits for them, and re-layouts: 9.12 us -> none  [the longest x1 7.27 us: mixer_half(): within_block + carried_part]
    unnamed x27 -> x20, local copies, waits for them, and re-layouts: 13.4 us -> 5.21 us
  transfers between devices with their start and end apart: 5 -> 9, of which waited for: 2 -> 5; matrix products, arithmetic and copies ran while one was open for 53% -> 2% of each run, Pallas kernels for 0% -> 35%
where the time goes in v1:
time: 169 us; the launch traced here: 167 us
  Pallas kernels  63.6 us (38%)
  waiting for transfers between devices  37.9 us (22%)
  blocking collectives  37.4 us (22%)
  starting transfers between devices  19.6 us (12%)
  local copies, waits for them, and re-layouts  6.61 us (4%)
    all_to_all x2, blocking collectives, exchange(): return lax.all_to_all(x, axis, split_axis=0, concat_axis=0, tiled=True)  37.4 us
    all_to_all x4, waiting for transfers between devices, exchange(): return lax.all_to_all(x, axis, split_axis=0, concat_axis=0, tiled=True)  20.8 us
    ppermute x2, waiting for transfers between devices, to_chip(): lax.ppermute(x, 'tp', [(i, (i + 2 * shift) % lanes) for i in range(lanes)])  17.1 us
    all_to_all x4, starting transfers between devices, exchange(): return lax.all_to_all(x, axis, split_axis=0, concat_axis=0, tiled=True)  16 us
    pallas_call x1, Pallas kernels, retention(): pl.pallas_call(functools.partial(retention_kernel, slices), grid_spec=plt...  14.6 us
    pallas_call x1, Pallas kernels, expert_up(): pl.pallas_call(functools.partial(up_kernel, count), grid=(width // tile,)...  13.2 us
    pallas_call x1, Pallas kernels, project(): pl.pallas_call(functools.partial(project_kernel, lanes, heads), grid=(wid...  10.4 us
    pallas_call x1, Pallas kernels, expert_down(): pl.pallas_call(down_kernel, grid=(width // tile,), in_specs=[pl.BlockSpec...  9.66 us
  transfers between devices with their start and end apart: 9, of which 5 were waited for; matrix products, arithmetic and copies ran while one was open for 2% of the time, Pallas kernels for 35%

profile of v1, /device:TPU:0, one launch (start us, length us, event | category | flops | bytes accessed | tf_op | source)
XLA Modules:
  0.0 167.2 jit_solution(14818703868157756969)
XLA Ops:
  0.6 1.4 copy.20.ids_ref
  2.0 2.2 %dispatch.1 = bf16[128,2048]{1,0:T(8,128)(2,1)} custom-call(bf16[32,2048]{1,0:T(8,128)(2,1)} %x_ref.1, s32[32,2]{1,0:T(8,128)} %copy.20.ids_ref, f32[1,2048]{1,0:T(1,128)} %bitcast.21), custom_call_target="tpu_custom_call" | custom-call | flops 16777216 | bytes 524288 | tf_op jit(solution)/shard_map/dispatch/pallas_call | solution.py:260
  4.2 21.8 %all_to_all.42 = bf16[8,16,2048]{2,1,0:T(8,128)(2,1)S(1)} all-to-all(bf16[8,16,2048]{2,1,0:T(8,128)(2,1)} %bitcast.16), channel_id=1, replica_groups=mesh['ep'=8,'tp'=4] {'ep'}, dimensions={0} | all-to-all | bytes 1048576 | tf_op jit(solution)/shard_map/all_to_all | solution.py:353
  26.0 1.5 collective-permute-start
  27.6 1.4 pad.4.l_ref
  28.9 9.7 %collective-permute-done.refs_1_ = bf16[128,2048]{1,0:T(8,128)(2,1)S(1)} collective-permute-done((bf16[128,2048]{1,0:T(8,128)(2,1)S(1)}, bf16[128,2048]{1,0:T(8,128)(2,1)S(1)}, u32[]{:S(2)}, u32[]{:S(2)}) %collective-permute-start) | collective-permute-done | bytes 524320 | tf_op jit(solution)/shard_map/ppermute | solution.py:361
  38.6 14.6 %retention.1 = (f32[2048,512]{1,0:T(8,128)}, bf16[2048,512]{1,0:T(8,128)(2,1)}, bf16[8,80,256]{2,1,0:T(8,128)(2,1)}) custom-call(s32[1]{0:T(128)} %bitcast.place_ref, bf16[2048,512]{1,0:T(8,128)(2,1)} %q_ref.1, bf16[2048,512]{1,0:T(8,128)(2,1)} %k_ref.1, bf16[2048,512]{1,0:T(8,128)(2,1)} %v_ref.1, f32[8,2048]{1,0:T(8,128)} %pad.4.l_ref, ...), custom_call_target="tpu_custom_call" | custom-call | flops 6442450944 | bytes 12582912 | tf_op jit(solution)/shard_map/retention/pallas_call | solution.py:129
  53.2 4.4 %all-to-all-start = ((bf16[8,80,256]{2,1,0:T(8,128)(2,1)}), bf16[8,80,256]{2,1,0:T(8,128)(2,1)S(1)}, u32[]{:S(2)}, u32[]{:S(2)}) async-start(bf16[8,80,256]{2,1,0:T(8,128)(2,1)} %get-tuple-element.9), calls=%async_computation | async-start | bytes 655360 | tf_op jit(solution)/shard_map/all_to_all | solution.py:353
  59.2 13.2 %expert_up.1.h_ref = bf16[512,1792]{1,0:T(8,128)(2,1)} custom-call(bf16[128,2048]{1,0:T(8,128)(2,1)} %bitcast.19, bf16[128,2048]{1,0:T(8,128)(2,1)} %copy-done.6, bf16[128,2048]{1,0:T(8,128)(2,1)} %copy-done.7, bf16[128,2048]{1,0:T(8,128)(2,1)} %copy-done.8, bf16[1,2048,1792]{2,1,0:T(8,128)(2,1)} %refs_4_.1, bf16[1,2048,1792]{2,1,0:T(8,128)(2,1)} %refs_5_.1), custom_call_target="tpu_custom_call" | custom-call | flops 7516192768 | bytes 14680064 | tf_op jit(solution)/shard_map/expert_up/pallas_call | solution.py:312
  72.5 9.7 %expert_down.1 = (bf16[256,2048]{1,0:T(8,128)(2,1)}, bf16[256,2048]{1,0:T(8,128)(2,1)}) custom-call(bf16[512,1792]{1,0:T(8,128)(2,1)} %expert_up.1.h_ref, bf16[1,1792,2048]{2,1,0:T(8,128)(2,1)} %w_ref.2), custom_call_target="tpu_custom_call" | custom-call | flops 3758096384 | bytes 7340032 | tf_op jit(solution)/shard_map/expert_down/pallas_call | solution.py:337
  82.9 1.8 %prefix.1 = bf16[8,64,256]{2,1,0:T(8,128)(2,1)} custom-call(bf16[8,80,256]{2,1,0:T(8,128)(2,1)} %copy-done.1), custom_call_target="tpu_custom_call" | custom-call | flops 327680 | bytes 655360 | tf_op jit(solution)/shard_map/prefix/pallas_call | solution.py:166
  84.7 15.6 %all_to_all.43 = bf16[8,64,256]{2,1,0:T(8,128)(2,1)} all-to-all(bf16[8,64,256]{2,1,0:T(8,128)(2,1)} %prefix.1), channel_id=1, replica_groups=mesh['ep'=8,'tp'=4] {'ep'}, dimensions={0} | all-to-all | bytes 524288 | tf_op jit(solution)/shard_map/all_to_all | solution.py:353
  100.3 4.7 %finish.2 = bf16[2048,256]{1,0:T(8,128)(2,1)} custom-call(f32[2048,512]{1,0:T(8,128)} %get-tuple-element.7.local_ref, bf16[2048,512]{1,0:T(8,128)(2,1)} %get-tuple-element.8.qd_ref, bf16[2,256,256]{2,1,0:T(8,128)(2,1)} %bitcast.13, bf16[2048,512]{1,0:T(8,128)(2,1)} %gate_ref.3, f32[1,512]{1,0:T(1,128)} %bitcast.22), custom_call_target="tpu_custom_call" | custom-call | flops 268435456 | bytes 5242880 | tf_op jit(solution)/shard_map/finish/pallas_call | solution.py:186
  105.0 4.4 %all-to-all-start.2 = ((bf16[4,512,256]{2,1,0:T(8,128)(2,1)}), bf16[4,512,256]{2,1,0:T(8,128)(2,1)}, u32[]{:S(2)}, u32[]{:S(2)}) async-start(bf16[4,512,256]{2,1,0:T(8,128)(2,1)} %bitcast.11), calls=%async_computation.2 | async-start | bytes 2097152 | tf_op jit(solution)/shard_map/all_to_all | solution.py:353
  109.9 2.0 %collective-permute-start.4 = (bf16[128,2048]{1,0:T(8,128)(2,1)S(1)}, bf16[128,2048]{1,0:T(8,128)(2,1)S(1)}, u32[]{:S(2)}, u32[]{:S(2)}) collective-permute-start(bf16[128,2048]{1,0:T(8,128)(2,1)S(1)} %slice.11), channel_id=1, source_target_pairs={{0,2},{1,3},{2,0},{3,1},{4,6},{5,7},{6,4},{7,5},{8,10},{9,11},{10,... | collective-permute-start | bytes 1572872 | tf_op jit(solution)/shard_map/ppermute | solution.py:361
  111.9 4.7 %finish.3 = bf16[2048,256]{1,0:T(8,128)(2,1)} custom-call(f32[2048,512]{1,0:T(8,128)} %get-tuple-element.7.local_ref, bf16[2048,512]{1,0:T(8,128)(2,1)} %get-tuple-element.8.qd_ref, bf16[2,256,256]{2,1,0:T(8,128)(2,1)} %bitcast.14, bf16[2048,512]{1,0:T(8,128)(2,1)} %gate_ref.3, f32[1,512]{1,0:T(1,128)} %bitcast.23), custom_call_target="tpu_custom_call" | custom-call | flops 268435456 | bytes 5242880 | tf_op jit(solution)/shard_map/finish/pallas_call | solution.py:186
  116.6 7.9 %all-to-all-done.2.refs_0_ = bf16[4,512,256]{2,1,0:T(8,128)(2,1)} async-done(((bf16[4,512,256]{2,1,0:T(8,128)(2,1)}), bf16[4,512,256]{2,1,0:T(8,128)(2,1)}, u32[]{:S(2)}, u32[]{:S(2)}) %all-to-all-start.2) | async-done | bytes 1048608 | tf_op jit(solution)/shard_map/all_to_all | solution.py:353
  124.5 3.6 %all-to-all-start.3 = ((bf16[4,512,256]{2,1,0:T(8,128)(2,1)}), bf16[4,512,256]{2,1,0:T(8,128)(2,1)S(1)}, u32[]{:S(2)}, u32[]{:S(2)}) async-start(bf16[4,512,256]{2,1,0:T(8,128)(2,1)} %bitcast.12), calls=%async_computation.3 | async-start | bytes 2097152 | tf_op jit(solution)/shard_map/all_to_all | solution.py:353
  128.2 7.5 %collective-permute-done.4 = bf16[128,2048]{1,0:T(8,128)(2,1)S(1)} collective-permute-done((bf16[128,2048]{1,0:T(8,128)(2,1)S(1)}, bf16[128,2048]{1,0:T(8,128)(2,1)S(1)}, u32[]{:S(2)}, u32[]{:S(2)}) %collective-permute-start.4) | collective-permute-done | bytes 524320 | tf_op jit(solution)/shard_map/ppermute | solution.py:361
  136.6 9.7 %all-to-all-done.3.refs_1_ = bf16[4,512,256]{2,1,0:T(8,128)(2,1)S(1)} async-done(((bf16[4,512,256]{2,1,0:T(8,128)(2,1)}), bf16[4,512,256]{2,1,0:T(8,128)(2,1)S(1)}, u32[]{:S(2)}, u32[]{:S(2)}) %all-to-all-start.3) | async-done | bytes 1048608 | tf_op jit(solution)/shard_map/all_to_all | solution.py:353
  146.3 3.6 %all-to-all-start.5 = ((bf16[8,16,2048]{2,1,0:T(8,128)(2,1)}), bf16[8,16,2048]{2,1,0:T(8,128)(2,1)S(1)}, u32[]{:S(2)}, u32[]{:S(2)}) async-start(bf16[8,16,2048]{2,1,0:T(8,128)(2,1)} %bitcast.9), calls=%async_computation.5 | async-start | bytes 1048576 | tf_op jit(solution)/shard_map/all_to_all | solution.py:353
  150.6 10.4 %project.1 = bf16[512,2048]{1,0:T(8,128)(2,1)} custom-call(bf16[4,512,256]{2,1,0:T(8,128)(2,1)} %all-to-all-done.2.refs_0_, bf16[4,512,256]{2,1,0:T(8,128)(2,1)} %copy-done.3, bf16[2048,2048]{1,0:T(8,128)(2,1)} %refs_2_.1), custom_call_target="tpu_custom_call" | custom-call | flops 4294967296 | bytes 10485760 | tf_op jit(solution)/shard_map/project/pallas_call | solution.py:219
  161.0 3.2 %all-to-all-done.5 = bf16[8,16,2048]{2,1,0:T(8,128)(2,1)S(1)} async-done(((bf16[8,16,2048]{2,1,0:T(8,128)(2,1)}), bf16[8,16,2048]{2,1,0:T(8,128)(2,1)S(1)}, u32[]{:S(2)}, u32[]{:S(2)}) %all-to-all-start.5) | async-done | bytes 524320 | tf_op jit(solution)/shard_map/all_to_all | solution.py:353
  165.0 2.2 %combine.1 = bf16[32,2048]{1,0:T(8,128)(2,1)} custom-call(bf16[128,2048]{1,0:T(8,128)(2,1)} %bitcast.15, s32[32,2]{1,0:T(8,128)} %copy.20.ids_ref, f32[32,2]{1,0:T(8,128)} %copy.22.w_ref), custom_call_target="tpu_custom_call" | custom-call | flops 52428800 | bytes 1048576 | tf_op jit(solution)/shard_map/combine/pallas_call | solution.py:282
  (29 shorter events, 5.3 us)
Async XLA Ops:
  26.0 27.2 %copy-start.4 = (bf16[8,16,2048]{2,1,0:T(8,128)(2,1)}, bf16[8,16,2048]{2,1,0:T(8,128)(2,1)S(1)}, u32[]{:S(2)}) copy-start(bf16[8,16,2048]{2,1,0:T(8,128)(2,1)S(1)} %all_to_all.42) | copy-start | bytes 1572868
  26.0 12.5 %collective-permute-start = (bf16[128,2048]{1,0:T(8,128)(2,1)S(1)}, bf16[128,2048]{1,0:T(8,128)(2,1)S(1)}, u32[]{:S(2)}, u32[]{:S(2)}) collective-permute-start(bf16[128,2048]{1,0:T(8,128)(2,1)S(1)} %bitcast.17), channel_id=1, source_target_pairs={{0,2},{1,3},{2,0},{3,1},{4,6},{5,7},{6,4},{7,5},{8,10},{9,11},{10,... | collective-permute-start | bytes 1572872 | tf_op jit(solution)/shard_map/ppermute | solution.py:361
  28.9 28.7 %collective-permute-start.1 = (bf16[128,2048]{1,0:T(8,128)(2,1)S(1)}, bf16[128,2048]{1,0:T(8,128)(2,1)S(1)}, u32[]{:S(2)}, u32[]{:S(2)}) collective-permute-start(bf16[128,2048]{1,0:T(8,128)(2,1)S(1)} %bitcast.18), channel_id=1, source_target_pairs={{0,1},{1,0},{2,3},{3,2},{4,5},{5,4},{6,7},{7,6},{8,9},{9,8},{10,11... | collective-permute-start | bytes 1572872 | tf_op jit(solution)/shard_map/ppermute | solution.py:357
  38.6 14.6 %copy-start.6 = (bf16[128,2048]{1,0:T(8,128)(2,1)}, bf16[128,2048]{1,0:T(8,128)(2,1)S(1)}, u32[]{:S(2)}) copy-start(bf16[128,2048]{1,0:T(8,128)(2,1)S(1)} %collective-permute-done.refs_1_) | copy-start | bytes 1572868
  38.6 19.1 %collective-permute-start.2 = (bf16[128,2048]{1,0:T(8,128)(2,1)S(1)}, bf16[128,2048]{1,0:T(8,128)(2,1)S(1)}, u32[]{:S(2)}, u32[]{:S(2)}) collective-permute-start(bf16[128,2048]{1,0:T(8,128)(2,1)S(1)} %collective-permute-done.refs_1_), channel_id=1, source_target_pairs={{0,1},{1,0},{2,3},{3,2},{4,5},{5,4},{6,7},{7,6},{8,9},{9,8},{10,11... | collective-permute-start | bytes 1572872 | tf_op jit(solution)/shard_map/ppermute | solution.py:357
  53.2 28.9 %all-to-all-start = ((bf16[8,80,256]{2,1,0:T(8,128)(2,1)}), bf16[8,80,256]{2,1,0:T(8,128)(2,1)S(1)}, u32[]{:S(2)}, u32[]{:S(2)}) async-start(bf16[8,80,256]{2,1,0:T(8,128)(2,1)} %get-tuple-element.9), calls=%async_computation | async-start | bytes 655360 | tf_op jit(solution)/shard_map/all_to_all | solution.py:353
  57.6 0.8 copy-start.7
  58.4 0.8 copy-start.8
  82.1 27.3 %collective-permute-start.3 = (bf16[256,2048]{1,0:T(8,128)(2,1)}, bf16[256,2048]{1,0:T(8,128)(2,1)S(1)}, u32[]{:S(2)}, u32[]{:S(2)}) collective-permute-start(bf16[256,2048]{1,0:T(8,128)(2,1)} %get-tuple-element.11), channel_id=1, source_target_pairs={{0,1},{1,0},{2,3},{3,2},{4,5},{5,4},{6,7},{7,6},{8,9},{9,8},{10,11... | collective-permute-start | bytes 3145736 | tf_op jit(solution)/shard_map/ppermute | solution.py:357
  82.2 0.8 copy-start.1
  105.0 4.4 %copy-start.2 = (bf16[256,2048]{1,0:T(8,128)(2,1)S(1)}, bf16[256,2048]{1,0:T(8,128)(2,1)}, u32[]{:S(2)}) copy-start(bf16[256,2048]{1,0:T(8,128)(2,1)} %get-tuple-element.10) | copy-start | bytes 3145732
  105.0 19.5 %all-to-all-start.2 = ((bf16[4,512,256]{2,1,0:T(8,128)(2,1)}), bf16[4,512,256]{2,1,0:T(8,128)(2,1)}, u32[]{:S(2)}, u32[]{:S(2)}) async-start(bf16[4,512,256]{2,1,0:T(8,128)(2,1)} %bitcast.11), calls=%async_computation.2 | async-start | bytes 2097152 | tf_op jit(solution)/shard_map/all_to_all | solution.py:353
  109.9 25.7 %collective-permute-start.4 = (bf16[128,2048]{1,0:T(8,128)(2,1)S(1)}, bf16[128,2048]{1,0:T(8,128)(2,1)S(1)}, u32[]{:S(2)}, u32[]{:S(2)}) collective-permute-start(bf16[128,2048]{1,0:T(8,128)(2,1)S(1)} %slice.11), channel_id=1, source_target_pairs={{0,2},{1,3},{2,0},{3,1},{4,6},{5,7},{6,4},{7,5},{8,10},{9,11},{10,... | collective-permute-start | bytes 1572872 | tf_op jit(solution)/shard_map/ppermute | solution.py:361
  124.5 25.4 %copy-start.5 = (f32[32,2]{0,1:T(2,128)S(1)}, f32[32,2]{0,1:T(2,128)}, u32[]{:S(2)}) copy-start(f32[32,2]{0,1:T(2,128)} %param.27) | copy-start | bytes 772
  124.5 21.8 %all-to-all-start.3 = ((bf16[4,512,256]{2,1,0:T(8,128)(2,1)}), bf16[4,512,256]{2,1,0:T(8,128)(2,1)S(1)}, u32[]{:S(2)}, u32[]{:S(2)}) async-start(bf16[4,512,256]{2,1,0:T(8,128)(2,1)} %bitcast.12), calls=%async_computation.3 | async-start | bytes 2097152 | tf_op jit(solution)/shard_map/all_to_all | solution.py:353
  146.3 4.3 %copy-start.3 = (bf16[4,512,256]{2,1,0:T(8,128)(2,1)}, bf16[4,512,256]{2,1,0:T(8,128)(2,1)S(1)}, u32[]{:S(2)}) copy-start(bf16[4,512,256]{2,1,0:T(8,128)(2,1)S(1)} %all-to-all-done.3.refs_1_) | copy-start | bytes 3145732
  146.3 17.9 %all-to-all-start.5 = ((bf16[8,16,2048]{2,1,0:T(8,128)(2,1)}), bf16[8,16,2048]{2,1,0:T(8,128)(2,1)S(1)}, u32[]{:S(2)}, u32[]{:S(2)}) async-start(bf16[8,16,2048]{2,1,0:T(8,128)(2,1)} %bitcast.9), calls=%async_computation.5 | async-start | bytes 1048576 | tf_op jit(solution)/shard_map/all_to_all | solution.py:353
  164.2 0.8 copy-start

commit v2 on v1

--- a/solution.py
+++ b/solution.py
@@ -180,53 +180,55 @@
     out_ref[...] = (gate * retained * inverse_rms * gain_ref[...]).astype(BF16)
 
 
-def finish(head, local, q_decayed, incoming, mix_gate, ret_gain):
-    rows = local.shape[0]
-    tile = pl.BlockSpec((BLOCK, HEAD_DIM), lambda b: (b, head))
+def finish(local, q_decayed, incoming, mix_gate, ret_gain):
+    rows, width = local.shape
+    tile = pl.BlockSpec((BLOCK, HEAD_DIM), lambda h, b: (b, h))
     return pl.pallas_call(
         finish_kernel,
-        grid=(rows // BLOCK,),
+        grid=(width // HEAD_DIM, rows // BLOCK),
         in_specs=[
             tile, tile,
-            pl.BlockSpec((1, HEAD_DIM, HEAD_DIM), lambda b: (head, 0, 0)),
+            pl.BlockSpec((1, HEAD_DIM, HEAD_DIM), lambda h, b: (h, 0, 0)),
             tile,
-            pl.BlockSpec((1, HEAD_DIM), lambda b: (0, head)),
+            pl.BlockSpec((1, HEAD_DIM), lambda h, b: (0, h)),
         ],
-        out_specs=pl.BlockSpec((BLOCK, HEAD_DIM), lambda b: (b, 0)),
-        out_shape=jax.ShapeDtypeStruct((rows, HEAD_DIM), BF16),
-        compiler_params=params("arbitrary"),
-        cost_estimate=cost(rows * HEAD_DIM * HEAD_DIM * 2, rows * HEAD_DIM * 10),
+        out_specs=tile,
+        out_shape=jax.ShapeDtypeStruct((rows, width), BF16),
+        compiler_params=params("arbitrary", "arbitrary"),
+        cost_estimate=cost(rows * width * HEAD_DIM * 2, rows * width * 10),
         name="finish",
     )(local, q_decayed, incoming, mix_gate, ret_gain)
 
 
-def project_kernel(lanes, heads, *refs):
-    pieces, w_ref, out_ref = refs[:heads], refs[heads], refs[heads + 1]
-    total = None
-    for h in range(heads):
+def project_kernel(x_ref, w_ref, out_ref, x):
+    lanes, _, width = x_ref.shape
+
+    @pl.when(pl.program_id(0) == 0)
+    def _():
         for lane in range(lanes):
-            r0 = (lane * heads + h) * HEAD_DIM
-            term = dot(pieces[h][lane], w_ref[r0 : r0 + HEAD_DIM, :])
-            total = term if total is None else total + term
-    out_ref[...] = total.astype(BF16)
-
-
-def project(pieces, w_out):
-    heads = len(pieces)
-    lanes, rows, _ = pieces[0].shape
+            x[:, lane * width : (lane + 1) * width] = x_ref[lane]
+
+    out_ref[...] = dot(x[...], w_ref[...]).astype(BF16)
+
+
+def project(gathered, w_out):
+    lanes, rows, part = gathered.shape
     depth, width = w_out.shape
-    tile = 256
-    return pl.pallas_call(
-        functools.partial(project_kernel, lanes, heads),
+    tile = 512
+    return pl.pallas_call(
+        project_kernel,
         grid=(width // tile,),
-        in_specs=[pl.BlockSpec((lanes, rows, HEAD_DIM), lambda n: (0, 0, 0))] * heads
-        + [pl.BlockSpec((depth, tile), lambda n: (0, n))],
+        in_specs=[
+            pl.BlockSpec((lanes, rows, part), lambda n: (0, 0, 0)),
+            pl.BlockSpec((depth, tile), lambda n: (0, n)),
+        ],
         out_specs=pl.BlockSpec((rows, tile), lambda n: (0, n)),
         out_shape=jax.ShapeDtypeStruct((rows, width), BF16),
+        scratch_shapes=[pltpu.VMEM((rows, depth), BF16)],
         compiler_params=params("arbitrary"),
         cost_estimate=cost(2 * rows * depth * width, 2 * (rows * depth + depth * width)),
         name="project",
-    )(*pieces, w_out)
+    )(gathered, w_out)
 
 
 def slots_of(ids, capacity, count):
@@ -332,7 +334,7 @@
 def expert_down(hidden, w_down):
     rows, depth = hidden.shape
     width = w_down.shape[2]
-    tile = 256
+    tile = 512
     out = pl.BlockSpec((rows // 2, tile), lambda n: (0, n))
     return pl.pallas_call(
         down_kernel,
@@ -379,17 +381,19 @@
     local, q_decayed, message = retention(
         mix_query, mix_key, mix_value, log_decay, devices, place
     )
-    incoming = exchange(prefix(exchange(message, "ep")), "ep")
+    own, message = lax.optimization_barrier((own, message))
+    arrived = exchange(message, "ep")
+    starts = prefix(arrived)
+    incoming = exchange(starts, "ep")
     incoming = incoming.reshape(heads, HEAD_DIM, HEAD_DIM)
 
     near = [own] + [to_chip(own, s, lanes) for s in range(1, chips)]
     pieces = near + [to_core(x, lanes) for x in near]
 
     gain = ret_gain.reshape(1, -1)
-    gathered = []
-    for h in range(heads):
-        out = finish(h, local, q_decayed, incoming, mix_gate, gain)
-        gathered.append(exchange(out.reshape(lanes, -1, HEAD_DIM), "tp"))
+    mixed = finish(local, q_decayed, incoming, mix_gate, gain)
+    *pieces, mixed = lax.optimization_barrier((*pieces, mixed))
+    gathered = exchange(mixed.reshape(lanes, -1, mixed.shape[1]), "tp")
 
     hidden = expert_up(pieces, w_gate, w_up)
     keep, send = expert_down(hidden, w_down)
@@ -422,6 +426,7 @@
         P("ep", "tp", None),
     )
     out_specs = (P(("ep", "tp"), None), P(("ep", "tp"), None))
+
     return jax.shard_map(
         on_device, mesh=mesh, in_specs=in_specs, out_specs=out_specs, check_vma=False
     )

time: 169 us -> 159 us (0.941)
  blocking collectives: 37.4 us -> 15.4 us
  waiting for transfers between devices: 37.9 us -> 49.2 us
  Pallas kernels: 63.6 us -> 59 us
  starting transfers between devices: 19.6 us -> 24.2 us
    ppermute x2, waiting for transfers between devices: 17.1 us -> 44.4 us  [to_chip(): lax.ppermute(x, 'tp', [(i, (i + 2 * shift) % lanes) for i in range(lanes)])]
    all_to_all x2 -> x1, blocking collectives: 37.4 us -> 15.4 us  [exchange(): return lax.all_to_all(x, axis, split_axis=0, concat_axis=0, tiled=True)]
    all_to_all x4, waiting for transfers between devices: 20.8 us -> 4.74 us  [exchange(): return lax.all_to_all(x, axis, split_axis=0, concat_axis=0, tiled=True)]
    all_to_all x4, starting transfers between devices: 16 us -> 20.6 us  [exchange(): return lax.all_to_all(x, axis, split_axis=0, concat_axis=0, tiled=True)]
    pallas_call x3 -> x2, Pallas kernels: 19.8 us -> 17.1 us  [the longest x1 8.87 us: project(): pl.pallas_call(project_kernel, grid=(width // tile,), in_specs=[pl.BlockS...]
  transfers between devices with their start and end apart: 9 -> 9, of which waited for: 5 -> 3; matrix products, arithmetic and copies ran while one was open for 2% -> 3% of each run, Pallas kernels for 35% -> 21%
where the time goes in v2:
time: 159 us; the launch traced here: 158 us
  Pallas kernels  59 us (37%)
  waiting for transfers between devices  49.2 us (31%)
  starting transfers between devices  24.2 us (15%)
  blocking collectives  15.4 us (10%)
  local copies, waits for them, and re-layouts  6.58 us (4%)
  other arithmetic  2.52 us (2%)
    ppermute x2, waiting for transfers between devices, to_chip(): lax.ppermute(x, 'tp', [(i, (i + 2 * shift) % lanes) for i in range(lanes)])  44.4 us
    all_to_all x4, starting transfers between devices, exchange(): return lax.all_to_all(x, axis, split_axis=0, concat_axis=0, tiled=True)  20.6 us
    all_to_all x1, blocking collectives, exchange(): return lax.all_to_all(x, axis, split_axis=0, concat_axis=0, tiled=True)  15.4 us
    pallas_call x1, Pallas kernels, retention(): pl.pallas_call(functools.partial(retention_kernel, slices), grid_spec=plt...  14.5 us
    pallas_call x1, Pallas kernels, expert_up(): pl.pallas_call(functools.partial(up_kernel, count), grid=(width // tile,)...  13.2 us
    pallas_call x1, Pallas kernels, project(): pl.pallas_call(project_kernel, grid=(width // tile,), in_specs=[pl.BlockS...  8.87 us
    pallas_call x1, Pallas kernels, finish(): pl.pallas_call(finish_kernel, grid=(width // HEAD_DIM, rows // BLOCK), in...  8.24 us
    pallas_call x1, Pallas kernels, expert_down(): pl.pallas_call(down_kernel, grid=(width // tile,), in_specs=[pl.BlockSpec...  8 us
  transfers between devices with their start and end apart: 9, of which 3 were waited for; matrix products, arithmetic and copies ran while one was open for 3% of the time, Pallas kernels for 21%

profile of v2, /device:TPU:0, one launch (start us, length us, event | category | flops | bytes accessed | tf_op | source)
XLA Modules:
  0.0 157.6 jit_solution(9195804886543497791)
XLA Ops:
  0.6 1.4 copy.20.ids_ref
  2.0 2.2 %dispatch.1 = bf16[128,2048]{1,0:T(8,128)(2,1)} custom-call(bf16[32,2048]{1,0:T(8,128)(2,1)} %x_ref.1, s32[32,2]{1,0:T(8,128)} %copy.20.ids_ref, f32[1,2048]{1,0:T(1,128)} %bitcast.17), custom_call_target="tpu_custom_call" | custom-call | flops 16777216 | bytes 524288 | tf_op jit(solution)/shard_map/dispatch/pallas_call | solution.py:262
  4.2 7.3 %all-to-all-start = ((bf16[8,16,2048]{2,1,0:T(8,128)(2,1)}), bf16[8,16,2048]{2,1,0:T(8,128)(2,1)S(1)}, u32[]{:S(2)}, u32[]{:S(2)}) async-start(bf16[8,16,2048]{2,1,0:T(8,128)(2,1)} %bitcast.10), calls=%async_computation | async-start | bytes 1048576 | tf_op jit(solution)/shard_map/all_to_all | solution.py:355
  11.5 1.4 pad.4.l_ref
  12.9 14.5 %retention.1 = (f32[2048,512]{1,0:T(8,128)}, bf16[2048,512]{1,0:T(8,128)(2,1)}, bf16[8,80,256]{2,1,0:T(8,128)(2,1)}) custom-call(s32[1]{0:T(128)} %bitcast.3.place_ref, bf16[2048,512]{1,0:T(8,128)(2,1)} %q_ref.1, bf16[2048,512]{1,0:T(8,128)(2,1)} %k_ref.1, bf16[2048,512]{1,0:T(8,128)(2,1)} %v_ref.1, f32[8,2048]{1,0:T(8,128)} %pad.4.l_ref, ...), custom_call_target="tpu_custom_call" | custom-call | flops 6442450944 | bytes 12582912 | tf_op jit(solution)/shard_map/retention/pallas_call | solution.py:129
  27.3 6.0 %all-to-all-start.1 = ((bf16[8,80,256]{2,1,0:T(8,128)(2,1)}), bf16[8,80,256]{2,1,0:T(8,128)(2,1)S(1)}, u32[]{:S(2)}, u32[]{:S(2)}) async-start(bf16[8,80,256]{2,1,0:T(8,128)(2,1)} %get-tuple-element.18), calls=%async_computation.1 | async-start | bytes 655360 | tf_op jit(solution)/shard_map/all_to_all | solution.py:355
  33.4 1.5 collective-permute-start
  34.9 11.3 %collective-permute-done.refs_1_ = bf16[128,2048]{1,0:T(8,128)(2,1)S(1)} collective-permute-done((bf16[128,2048]{1,0:T(8,128)(2,1)S(1)}, bf16[128,2048]{1,0:T(8,128)(2,1)S(1)}, u32[]{:S(2)}, u32[]{:S(2)}) %collective-permute-start) | collective-permute-done | bytes 524320 | tf_op jit(solution)/shard_map/ppermute | solution.py:363
  47.0 1.7 %prefix.1 = bf16[8,64,256]{2,1,0:T(8,128)(2,1)} custom-call(bf16[8,80,256]{2,1,0:T(8,128)(2,1)} %copy-done.2), custom_call_target="tpu_custom_call" | custom-call | flops 327680 | bytes 655360 | tf_op jit(solution)/shard_map/prefix/pallas_call | solution.py:166
  48.7 15.4 %all_to_all.38 = bf16[8,64,256]{2,1,0:T(8,128)(2,1)} all-to-all(bf16[8,64,256]{2,1,0:T(8,128)(2,1)} %prefix.1), channel_id=1, replica_groups=mesh['ep'=8,'tp'=4] {'ep'}, dimensions={0} | all-to-all | bytes 524288 | tf_op jit(solution)/shard_map/all_to_all | solution.py:355
  64.1 8.2 %finish.1 = bf16[2048,512]{1,0:T(8,128)(2,1)} custom-call(f32[2048,512]{1,0:T(8,128)} %get-tuple-element.16.local_ref, bf16[2048,512]{1,0:T(8,128)(2,1)} %get-tuple-element.17.qd_ref, bf16[2,256,256]{2,1,0:T(8,128)(2,1)} %bitcast.12, bf16[2048,512]{1,0:T(8,128)(2,1)} %gate_ref.1, f32[1,512]{1,0:T(1,128)} %bitcast.18), custom_call_target="tpu_custom_call" | custom-call | flops 536870912 | bytes 10485760 | tf_op jit(solution)/shard_map/finish/pallas_call | solution.py:186
  73.1 0.8 copy-done.8
  73.9 13.2 %expert_up.1.h_ref = bf16[512,1792]{1,0:T(8,128)(2,1)} custom-call(bf16[128,2048]{1,0:T(8,128)(2,1)} %bitcast.15, bf16[128,2048]{1,0:T(8,128)(2,1)} %copy-done.6, bf16[128,2048]{1,0:T(8,128)(2,1)} %copy-done.7, bf16[128,2048]{1,0:T(8,128)(2,1)} %copy-done.8, bf16[1,2048,1792]{2,1,0:T(8,128)(2,1)} %refs_4_.1, bf16[1,2048,1792]{2,1,0:T(8,128)(2,1)} %refs_5_.1), custom_call_target="tpu_custom_call" | custom-call | flops 7516192768 | bytes 14680064 | tf_op jit(solution)/shard_map/expert_up/pallas_call | solution.py:314
  87.1 8.0 %expert_down.1 = (bf16[256,2048]{1,0:T(8,128)(2,1)}, bf16[256,2048]{1,0:T(8,128)(2,1)}) custom-call(bf16[512,1792]{1,0:T(8,128)(2,1)} %expert_up.1.h_ref, bf16[1,1792,2048]{2,1,0:T(8,128)(2,1)} %w_ref.4), custom_call_target="tpu_custom_call" | custom-call | flops 3758096384 | bytes 7340032 | tf_op jit(solution)/shard_map/expert_down/pallas_call | solution.py:339
  95.1 3.8 %all-to-all-start.3 = ((bf16[4,512,512]{2,1,0:T(8,128)(2,1)}), bf16[4,512,512]{2,1,0:T(8,128)(2,1)S(1)}, u32[]{:S(2)}, u32[]{:S(2)}) async-start(bf16[4,512,512]{2,1,0:T(8,128)(2,1)} %bitcast.7), calls=%async_computation.3 | async-start | bytes 4194304 | tf_op jit(solution)/shard_map/all_to_all | solution.py:355
  98.9 1.6 %add_convert_fusion = bf16[256,2048]{1,0:T(8,128)(2,1)S(1)} fusion(bf16[256,2048]{1,0:T(8,128)(2,1)} %collective-permute-done.3, bf16[256,2048]{1,0:T(8,128)(2,1)S(1)} %copy-done.3), kind=kLoop, calls=%fused_computation | loop fusion | flops 2097152 | bytes 3145728 | tf_op jit(solution)/shard_map/convert_element_type | solution.py:400
  100.5 2.0 %collective-permute-start.4 = (bf16[128,2048]{1,0:T(8,128)(2,1)S(1)}, bf16[128,2048]{1,0:T(8,128)(2,1)S(1)}, u32[]{:S(2)}, u32[]{:S(2)}) collective-permute-start(bf16[128,2048]{1,0:T(8,128)(2,1)S(1)} %slice.11), channel_id=1, source_target_pairs={{0,2},{1,3},{2,0},{3,1},{4,6},{5,7},{6,4},{7,5},{8,10},{9,11},{10,... | collective-permute-start | bytes 1572872 | tf_op jit(solution)/shard_map/ppermute | solution.py:363
  102.6 33.1 %collective-permute-done.4 = bf16[128,2048]{1,0:T(8,128)(2,1)S(1)} collective-permute-done((bf16[128,2048]{1,0:T(8,128)(2,1)S(1)}, bf16[128,2048]{1,0:T(8,128)(2,1)S(1)}, u32[]{:S(2)}, u32[]{:S(2)}) %collective-permute-start.4) | collective-permute-done | bytes 524320 | tf_op jit(solution)/shard_map/ppermute | solution.py:363
  135.7 0.9 add_convert_fusion.1
  136.6 3.6 %all-to-all-start.4 = ((bf16[8,16,2048]{2,1,0:T(8,128)(2,1)}), bf16[8,16,2048]{2,1,0:T(8,128)(2,1)S(1)}, u32[]{:S(2)}, u32[]{:S(2)}) async-start(bf16[8,16,2048]{2,1,0:T(8,128)(2,1)} %bitcast.8), calls=%async_computation.4 | async-start | bytes 1048576 | tf_op jit(solution)/shard_map/all_to_all | solution.py:355
  140.9 8.9 %project.1 = bf16[512,2048]{1,0:T(8,128)(2,1)} custom-call(bf16[4,512,512]{2,1,0:T(8,128)(2,1)} %copy-done, bf16[2048,2048]{1,0:T(8,128)(2,1)} %w_ref.3), custom_call_target="tpu_custom_call" | custom-call | flops 4294967296 | bytes 10485760 | tf_op jit(solution)/shard_map/project/pallas_call | solution.py:218
  149.8 4.7 %all-to-all-done.4 = bf16[8,16,2048]{2,1,0:T(8,128)(2,1)S(1)} async-done(((bf16[8,16,2048]{2,1,0:T(8,128)(2,1)}), bf16[8,16,2048]{2,1,0:T(8,128)(2,1)S(1)}, u32[]{:S(2)}, u32[]{:S(2)}) %all-to-all-start.4) | async-done | bytes 524320 | tf_op jit(solution)/shard_map/all_to_all | solution.py:355
  154.5 0.8 copy-done.1
  155.3 2.2 %combine.1 = bf16[32,2048]{1,0:T(8,128)(2,1)} custom-call(bf16[128,2048]{1,0:T(8,128)(2,1)} %bitcast.11, s32[32,2]{1,0:T(8,128)} %copy.20.ids_ref, f32[32,2]{1,0:T(8,128)} %copy.22.w_ref), custom_call_target="tpu_custom_call" | custom-call | flops 52428800 | bytes 1048576 | tf_op jit(solution)/shard_map/combine/pallas_call | solution.py:284
  (27 shorter events, 2.3 us)
Async XLA Ops:
  4.2 23.1 %all-to-all-start = ((bf16[8,16,2048]{2,1,0:T(8,128)(2,1)}), bf16[8,16,2048]{2,1,0:T(8,128)(2,1)S(1)}, u32[]{:S(2)}, u32[]{:S(2)}) async-start(bf16[8,16,2048]{2,1,0:T(8,128)(2,1)} %bitcast.10), calls=%async_computation | async-start | bytes 1048576 | tf_op jit(solution)/shard_map/all_to_all | solution.py:355
  27.3 45.0 %copy-start.4 = (bf16[8,16,2048]{2,1,0:T(8,128)(2,1)}, bf16[8,16,2048]{2,1,0:T(8,128)(2,1)S(1)}, u32[]{:S(2)}) copy-start(bf16[8,16,2048]{2,1,0:T(8,128)(2,1)S(1)} %all-to-all-done) | copy-start | bytes 1572868
  27.3 18.8 %all-to-all-start.1 = ((bf16[8,80,256]{2,1,0:T(8,128)(2,1)}), bf16[8,80,256]{2,1,0:T(8,128)(2,1)S(1)}, u32[]{:S(2)}, u32[]{:S(2)}) async-start(bf16[8,80,256]{2,1,0:T(8,128)(2,1)} %get-tuple-element.18), calls=%async_computation.1 | async-start | bytes 655360 | tf_op jit(solution)/shard_map/all_to_all | solution.py:355
  33.4 12.8 %collective-permute-start = (bf16[128,2048]{1,0:T(8,128)(2,1)S(1)}, bf16[128,2048]{1,0:T(8,128)(2,1)S(1)}, u32[]{:S(2)}, u32[]{:S(2)}) collective-permute-start(bf16[128,2048]{1,0:T(8,128)(2,1)S(1)} %bitcast.13), channel_id=1, source_target_pairs={{0,2},{1,3},{2,0},{3,1},{4,6},{5,7},{6,4},{7,5},{8,10},{9,11},{10,... | collective-permute-start | bytes 1572872 | tf_op jit(solution)/shard_map/ppermute | solution.py:363
  34.9 37.4 %collective-permute-start.1 = (bf16[128,2048]{1,0:T(8,128)(2,1)S(1)}, bf16[128,2048]{1,0:T(8,128)(2,1)S(1)}, u32[]{:S(2)}, u32[]{:S(2)}) collective-permute-start(bf16[128,2048]{1,0:T(8,128)(2,1)S(1)} %bitcast.14), channel_id=1, source_target_pairs={{0,1},{1,0},{2,3},{3,2},{4,5},{5,4},{6,7},{7,6},{8,9},{9,8},{10,11... | collective-permute-start | bytes 1572872 | tf_op jit(solution)/shard_map/ppermute | solution.py:359
  46.2 26.1 %copy-start.6 = (bf16[128,2048]{1,0:T(8,128)(2,1)}, bf16[128,2048]{1,0:T(8,128)(2,1)S(1)}, u32[]{:S(2)}) copy-start(bf16[128,2048]{1,0:T(8,128)(2,1)S(1)} %collective-permute-done.refs_1_) | copy-start | bytes 1572868
  46.2 26.1 %collective-permute-start.2 = (bf16[128,2048]{1,0:T(8,128)(2,1)S(1)}, bf16[128,2048]{1,0:T(8,128)(2,1)S(1)}, u32[]{:S(2)}, u32[]{:S(2)}) collective-permute-start(bf16[128,2048]{1,0:T(8,128)(2,1)S(1)} %collective-permute-done.refs_1_), channel_id=1, source_target_pairs={{0,1},{1,0},{2,3},{3,2},{4,5},{5,4},{6,7},{7,6},{8,9},{9,8},{10,11... | collective-permute-start | bytes 1572872 | tf_op jit(solution)/shard_map/ppermute | solution.py:359
  46.2 0.8 copy-start.2
  72.3 0.8 copy-start.7
  73.1 0.8 copy-start.8
  95.1 3.8 %collective-permute-start.3 = (bf16[256,2048]{1,0:T(8,128)(2,1)}, bf16[256,2048]{1,0:T(8,128)(2,1)}, u32[]{:S(2)}, u32[]{:S(2)}) collective-permute-start(bf16[256,2048]{1,0:T(8,128)(2,1)} %get-tuple-element.25), channel_id=1, source_target_pairs={{0,1},{1,0},{2,3},{3,2},{4,5},{5,4},{6,7},{7,6},{8,9},{9,8},{10,11... | collective-permute-start | bytes 3145736 | tf_op jit(solution)/shard_map/ppermute | solution.py:359
  95.1 3.8 %copy-start.3 = (bf16[256,2048]{1,0:T(8,128)(2,1)S(1)}, bf16[256,2048]{1,0:T(8,128)(2,1)}, u32[]{:S(2)}) copy-start(bf16[256,2048]{1,0:T(8,128)(2,1)} %get-tuple-element.24) | copy-start | bytes 3145732
  95.1 41.5 %all-to-all-start.3 = ((bf16[4,512,512]{2,1,0:T(8,128)(2,1)}), bf16[4,512,512]{2,1,0:T(8,128)(2,1)S(1)}, u32[]{:S(2)}, u32[]{:S(2)}) async-start(bf16[4,512,512]{2,1,0:T(8,128)(2,1)} %bitcast.7), calls=%async_computation.3 | async-start | bytes 4194304 | tf_op jit(solution)/shard_map/all_to_all | solution.py:355
  100.5 39.8 %copy-start.5 = (f32[32,2]{0,1:T(2,128)S(1)}, f32[32,2]{0,1:T(2,128)}, u32[]{:S(2)}) copy-start(f32[32,2]{0,1:T(2,128)} %param.27) | copy-start | bytes 772
  100.5 35.2 %collective-permute-start.4 = (bf16[128,2048]{1,0:T(8,128)(2,1)S(1)}, bf16[128,2048]{1,0:T(8,128)(2,1)S(1)}, u32[]{:S(2)}, u32[]{:S(2)}) collective-permute-start(bf16[128,2048]{1,0:T(8,128)(2,1)S(1)} %slice.11), channel_id=1, source_target_pairs={{0,2},{1,3},{2,0},{3,1},{4,6},{5,7},{6,4},{7,5},{8,10},{9,11},{10,... | collective-permute-start | bytes 1572872 | tf_op jit(solution)/shard_map/ppermute | solution.py:363
  136.6 4.3 %copy-start = (bf16[4,512,512]{2,1,0:T(8,128)(2,1)}, bf16[4,512,512]{2,1,0:T(8,128)(2,1)S(1)}, u32[]{:S(2)}) copy-start(bf16[4,512,512]{2,1,0:T(8,128)(2,1)S(1)} %all-to-all-done.3.x_ref) | copy-start | bytes 6291460
  136.6 17.9 %all-to-all-start.4 = ((bf16[8,16,2048]{2,1,0:T(8,128)(2,1)}), bf16[8,16,2048]{2,1,0:T(8,128)(2,1)S(1)}, u32[]{:S(2)}, u32[]{:S(2)}) async-start(bf16[8,16,2048]{2,1,0:T(8,128)(2,1)} %bitcast.8), calls=%async_computation.4 | async-start | bytes 1048576 | tf_op jit(solution)/shard_map/all_to_all | solution.py:355
  154.5 0.8 copy-start.1
